TPU v7x, 256 devices: a whole 4x4x8 slice. The times are simulated.
256 devices in a mesh: sp: 32 (over z, x), fs: 4 (over y), tp: 2 (over core).
Axes of the slice: x: 4, y: 4, z: 8, core: 2. Of those that a mesh axis runs over, the one named last changes fastest.
Arguments:
- inputs: bfloat16 [4, 4096, 2048], P('fs', 'sp'), may hold values from -6 to 6
- input_norm_gain: bfloat16 [2048], replicated, may hold values from 0.099609375 to 1.8984375
- receptance_matrix: bfloat16 [2048, 1024], P('fs', 'tp'), may hold values from -0.125 to 0.125
- key_matrix: bfloat16 [2048, 1024], P('fs', 'tp'), may hold values from -0.125 to 0.125
- value_matrix: bfloat16 [2048, 1024], P('fs', 'tp'), may hold values from -0.125 to 0.125
- pooling_input_weight: bfloat16 [2048, 1024], P('fs', 'tp'), may hold values from -0.125 to 0.125
- decay_lower_matrix: bfloat16 [2048, 128], replicated, may hold values from -0.125 to 0.125
- decay_raise_matrix: bfloat16 [2, 64, 1024], P(None, None, 'tp'), may hold values from -1 to 1
- decay_offset_bias: float32 [2, 1024], P(None, 'tp'), may hold values from -13 to -3
- removal_lower_matrix: bfloat16 [2048, 128], replicated, may hold values from -0.125 to 0.125
- removal_raise_matrix: bfloat16 [2, 64, 1024], P(None, None, 'tp'), may hold values from -1 to 1
- removal_rate_bias: float32 [2, 1024], P(None, 'tp'), may hold values from -9 to 1.5
- tempo_scale: float32 [4, 2, 16, 4096], P('fs', None, 'tp', 'sp'), may hold values from 0.3 to 3.2, as said below
- sudden_decay_extra: float32 [4, 2, 16, 4096], P('fs', None, 'tp', 'sp'), may hold values from -2.8 to 0
- head_norm_gain: bfloat16 [1024], P('tp'), may hold values from 0.099609375 to 1.8984375
- group_mixing_weight: bfloat16 [4, 256, 256], P('tp'), may hold values from -0.375 to 0.375
- attention_output_matrix: bfloat16 [2048, 1024], P('fs', 'tp'), may hold values from -0.125 to 0.125
- pooling_output_matrix: bfloat16 [2048, 1024], P('fs', 'tp'), may hold values from -0.125 to 0.125
Outputs:
- mixed_out: bfloat16 [4, 4096, 2048], P('fs', ('sp', 'tp'))
Inputs may be any that keep to these rules, and one draw needn't show every extreme that they name: `tempo_scale`: positive.
All inputs are finite; a program needn't handle non-finite values.
Results may differ from a plain program's by a relative error of at most 0.017.
Values may be sent and summed in bfloat16 or wider, within the bound.
No kernel may reach another device: no remote copies, remote signals or barrier semaphores. Data moves between devices by JAX's collectives and lax.ppermute only.
A program may use at most 128 MiB of HBM per device.

v0:
```python
import jax
import jax.numpy as jnp
from jax import lax
from jax.sharding import Mesh
from jax.sharding import PartitionSpec as P

HEAD = 64
DECAY_RANK = 64
RATE_RANK = 64
POOL_GROUPS = 4
GROUP_WIDTH = 256
SP = ("sp_0", "sp_1")
SP_TP = ("sp_0", "sp_1", "tp")
norm_eps = 1e-06
head_eps = 0.00064
unit_eps = 1e-06
span_len = 32
highest = lax.Precision.HIGHEST


def filled_with(shard, identity):
    return jax.tree.map(
        lambda a, e: jnp.broadcast_to(jnp.asarray(e, a.dtype), a.shape), shard, identity
    )


def prefix_by_axis(shard, axes, combine, identity, reverse):
    before = start = filled_with(shard, identity)
    total = shard
    for axis in reversed(axes):
        peers, here = (lax.axis_size(axis), lax.axis_index(axis))
        pieces = jax.tree.map(
            lambda part, kind: lax.all_gather(part.astype(kind), axis),
            total,
            (jnp.bfloat16, jnp.bfloat16),
        )
        inside, total = (start, start)
        for k in reversed(range(peers)) if reverse else range(peers):
            passed = k > here if reverse else k < here
            total = combine(
                total, jax.tree.map(lambda part, own: part[k].astype(own.dtype), pieces, shard)
            )
            inside = jax.tree.map(lambda new, old: jnp.where(passed, new, old), total, inside)
        before = combine(inside, before)
    return before


def with_halo(cells, sides, width):
    for axis, dim in sides:
        count = lax.axis_size(axis)
        ends = count - 1
        head = lax.slice_in_dim(cells, 0, width, axis=dim)
        tail = lax.slice_in_dim(cells, cells.shape[dim] - width, cells.shape[dim], axis=dim)
        cells = jnp.concatenate(
            [
                lax.ppermute(tail, axis, [(i, (i + 1) % count) for i in range(ends)]),
                cells,
                lax.ppermute(head, axis, [((i + 1) % count, i) for i in range(ends)]),
            ],
            axis=dim,
        )
    return cells


def contract(form, left, right):
    return jnp.einsum(form, left, right, precision=highest)


def matmul(left, right):
    return contract("...ij,...jk->...ik", left, right)


def project(left, weight):
    return jnp.dot(left, weight, preferred_element_type=jnp.float32).astype(jnp.bfloat16)


def against(row_block, weight):
    return lax.dot_general(
        row_block, weight, (((1,), (1,)), ((), ())), preferred_element_type=jnp.float32
    )


def chain_combine(earlier, later):
    return (matmul(earlier[0], later[0]), matmul(earlier[1], later[0]) + later[1])


def unit_inverse(lower):
    result = jnp.eye(lower.shape[-1], dtype=jnp.float32) - lower
    power = lower
    for level in range(4):
        power = matmul(power, power)
        result = result + matmul(result, power)
    return result


def span_terms(logarithm_decay, unit, removal, written, value, recept):
    inner = jnp.cumsum(logarithm_decay, axis=-2)
    last = inner[..., -1:, :]
    ahead = unit * jnp.exp(inner - logarithm_decay)
    shrink = jnp.exp(-inner)
    remove_scaled = removal * shrink
    write_scaled = written * shrink
    query = recept * jnp.exp(inner)
    spots = jnp.arange(span_len)
    strict = spots[:, None] > spots[None, :]
    within = spots[:, None] >= spots[None, :]
    link_remove = jnp.where(strict, contract("...tk,...sk->...ts", ahead, remove_scaled), 0.0)
    link_write = jnp.where(strict, contract("...tk,...sk->...ts", ahead, write_scaled), 0.0)
    read_remove = jnp.where(within, contract("...tk,...sk->...ts", query, remove_scaled), 0.0)
    read_write = jnp.where(within, contract("...tk,...sk->...ts", query, write_scaled), 0.0)
    inverse = unit_inverse(link_remove)
    pull_map = -matmul(inverse, ahead)
    pull_base = -matmul(inverse, matmul(link_write, value))
    tail = jnp.exp(last - inner)
    remove_tail = removal * tail
    write_tail = written * tail
    transfer = jnp.eye(unit.shape[-1], dtype=jnp.float32) * jnp.exp(last) + contract(
        "...sk,...sj->...kj", pull_map, remove_tail
    )
    carried = contract("...sv,...sk->...vk", pull_base, remove_tail) + contract(
        "...sv,...sk->...vk", value, write_tail
    )
    query_eff = query + matmul(read_remove, pull_map)
    local_read = matmul(read_remove, pull_base) + matmul(read_write, value)
    return (query_eff, local_read, transfer, carried)


def shards(
    inputs,
    input_norm_gain,
    receptance_matrix,
    key_matrix,
    value_matrix,
    pooling_input_weight,
    decay_lower_matrix,
    decay_raise_matrix,
    decay_offset_bias,
    removal_lower_matrix,
    removal_raise_matrix,
    removal_rate_bias,
    tempo_scale,
    sudden_decay_extra,
    head_norm_gain,
    group_mixing_weight,
    attention_output_matrix,
    pooling_output_matrix,
):
    recept_full, key_full, value_full, pool_full, attn_full, pool_back = (
        lax.all_gather(receptance_matrix, "fs", axis=0, tiled=True),
        lax.all_gather(key_matrix, "fs", axis=0, tiled=True),
        lax.all_gather(value_matrix, "fs", axis=0, tiled=True),
        lax.all_gather(pooling_input_weight, "fs", axis=0, tiled=True),
        lax.all_gather(attention_output_matrix, "fs", axis=0, tiled=True),
        lax.all_gather(pooling_output_matrix, "fs", axis=0, tiled=True),
    )
    row_block = inputs[0].astype(jnp.float32)
    normed = (
        row_block
        * lax.rsqrt(jnp.mean(row_block * row_block, axis=-1, keepdims=True) + norm_eps)
        * input_norm_gain.astype(jnp.float32)
    ).astype(jnp.bfloat16)
    tokens = normed.shape[0]
    heads = recept_full.shape[1] // HEAD
    blocks = tokens // span_len
    receptance = project(normed, recept_full).astype(jnp.float32).reshape(tokens, heads, HEAD)
    key_rows = project(normed, key_full).astype(jnp.float32).reshape(tokens, heads, HEAD)
    val_rows = project(normed, value_full).astype(jnp.float32).reshape(tokens, heads, HEAD)
    pool_in = project(normed, pool_full)
    decay_act = jnp.tanh(project(normed, decay_lower_matrix).astype(jnp.float32)).astype(
        jnp.bfloat16
    )
    rate_latent = project(normed, removal_lower_matrix)
    unit_keys = key_rows * lax.rsqrt(
        jnp.sum(key_rows * key_rows, axis=-1, keepdims=True) + unit_eps
    )
    decays = []
    removals = []
    writes = []
    for travel_direction in range(2):
        part = decay_act[:, travel_direction * DECAY_RANK : (travel_direction + 1) * DECAY_RANK]
        decay_pre = decay_offset_bias[travel_direction] + jnp.dot(
            part, decay_raise_matrix[travel_direction], preferred_element_type=jnp.float32
        )
        decay_velocity = jnp.exp(-jax.nn.softplus(-decay_pre) - 0.5).reshape(tokens, heads, HEAD)
        decays.append(
            -decay_velocity * tempo_scale[0, travel_direction].T[:, :, None]
            + sudden_decay_extra[0, travel_direction].T[:, :, None]
        )
        latent = rate_latent[:, travel_direction * RATE_RANK : (travel_direction + 1) * RATE_RANK]
        rate = jax.nn.sigmoid(
            removal_rate_bias[travel_direction]
            + jnp.dot(
                latent, removal_raise_matrix[travel_direction], preferred_element_type=jnp.float32
            )
        )
        rate = rate.reshape(tokens, heads, HEAD)
        removals.append(unit_keys * rate)
        writes.append(key_rows * rate)

    def both_ways(forward, backward):
        stacked = jnp.stack([forward, jnp.flip(backward, axis=0)], axis=0)
        return stacked.reshape(2, blocks, span_len, heads, HEAD).transpose(0, 3, 1, 2, 4)

    query_eff, local_read, transfer, carried = span_terms(
        both_ways(decays[0], decays[1]),
        both_ways(unit_keys, unit_keys),
        both_ways(removals[0], removals[1]),
        both_ways(writes[0], writes[1]),
        both_ways(val_rows, val_rows),
        both_ways(receptance, receptance),
    )
    prefix_map, prefix_sum = lax.associative_scan(chain_combine, (transfer, carried), axis=2)
    total_map = prefix_map[:, :, -1]
    total_sum = prefix_sum[:, :, -1]
    identity_map = jnp.broadcast_to(jnp.eye(HEAD, dtype=jnp.float32), total_map.shape[1:])
    empty = jnp.zeros(total_map.shape[1:], jnp.float32)
    ahead_in = prefix_by_axis(
        (total_map[0], total_sum[0]), SP, chain_combine, (identity_map, empty), False
    )
    behind_in = prefix_by_axis(
        (total_map[1], total_sum[1]), SP, chain_combine, (identity_map, empty), True
    )
    incoming = jnp.stack([ahead_in[1], behind_in[1]], axis=0)
    ending = matmul(incoming[:, :, None], prefix_map) + prefix_sum
    starting = jnp.concatenate([incoming[:, :, None], ending[:, :, :-1]], axis=2)
    reads = contract("...tk,...vk->...tv", query_eff, starting) + local_read
    reads = reads.transpose(0, 2, 3, 1, 4).reshape(2, tokens, heads, HEAD)
    readout = reads[0] + jnp.flip(reads[1], axis=0)
    centred = readout - jnp.mean(readout, axis=-1, keepdims=True)
    spread = jnp.mean(centred * centred, axis=-1, keepdims=True)
    attn_out = (centred * lax.rsqrt(spread + head_eps)).reshape(
        tokens, heads * HEAD
    ) * head_norm_gain.astype(jnp.float32)
    attn_out = attn_out.astype(jnp.bfloat16)
    reach = 2 ** (POOL_GROUPS - 1)
    rimmed = with_halo(pool_in, ((SP, 0),), reach).astype(jnp.float32)
    position = lax.axis_index(SP) * tokens + jnp.arange(tokens)
    length = tokens * lax.axis_size(SP)
    running = rimmed
    window_sums = []
    window_counts = []
    for level in range(POOL_GROUPS):
        shift = 2**level
        running = running[:-shift] + running[shift:]
        window_sums.append(running[reach - shift : reach - shift + tokens])
        upper = jnp.minimum(position + shift, length)
        lower = jnp.maximum(position - shift, 0)
        window_counts.append((upper - lower).astype(jnp.float32))
    window_sums = jnp.stack(window_sums, axis=0)
    window_counts = jnp.stack(window_counts, axis=0)
    pool_vals = pool_in.astype(jnp.float32)
    groups_here = pool_in.shape[1] // GROUP_WIDTH
    diffs = []
    for member in range(groups_here):
        group = lax.axis_index("tp") * groups_here + member
        chosen = lax.dynamic_index_in_dim(
            window_sums[:, :, member * GROUP_WIDTH : (member + 1) * GROUP_WIDTH],
            group,
            0,
            keepdims=False,
        )
        count = lax.dynamic_index_in_dim(window_counts, group, 0, keepdims=False)
        diffs.append(
            chosen / count[:, None]
            - pool_vals[:, member * GROUP_WIDTH : (member + 1) * GROUP_WIDTH]
        )
    pool_diff = jnp.concatenate(diffs, axis=1).astype(jnp.bfloat16)
    mixed = [
        jnp.dot(
            pool_diff[:, member * GROUP_WIDTH : (member + 1) * GROUP_WIDTH],
            group_mixing_weight[member],
            preferred_element_type=jnp.float32,
        )
        for member in range(groups_here)
    ]
    pool_out = jnp.concatenate(mixed, axis=1).astype(jnp.bfloat16)
    attn_half, pool_half = (
        lax.all_to_all(attn_out, "tp", split_axis=0, concat_axis=1, tiled=True),
        lax.all_to_all(pool_out, "tp", split_axis=0, concat_axis=1, tiled=True),
    )
    attn_whole, pool_whole = (
        lax.all_gather(attn_full, "tp", axis=1, tiled=True),
        lax.all_gather(pool_back, "tp", axis=1, tiled=True),
    )
    result = against(attn_half, attn_whole) + against(pool_half, pool_whole)
    return result.astype(jnp.bfloat16)[None]


def solution(mesh):
    split = Mesh(
        mesh.devices.reshape(8, 4, mesh.shape["fs"], mesh.shape["tp"]), ("sp_0", "sp_1", "fs", "tp")
    )
    in_specs = (
        P("fs", SP, None),
        P(),
        P("fs", "tp"),
        P("fs", "tp"),
        P("fs", "tp"),
        P("fs", "tp"),
        P(),
        P(None, None, "tp"),
        P(None, "tp"),
        P(),
        P(None, None, "tp"),
        P(None, "tp"),
        P("fs", None, "tp", SP),
        P("fs", None, "tp", SP),
        P("tp"),
        P("tp", None, None),
        P("fs", "tp"),
        P("fs", "tp"),
    )
    out_specs = P("fs", SP_TP, None)
    return jax.shard_map(
        shards, mesh=split, in_specs=in_specs, out_specs=out_specs, check_vma=False
    )
```

profile of v0, /device:TPU:7, one launch (start us, length us, event | category | flops | bytes accessed | tf_op | source)
XLA Modules:
  0.0 448.1 jit_solution(15655499817770157762)
XLA Ops:
  18.1 27.2 %all-gather.19.cloned.1.call-done = bf16[2048,512]{1,0:T(8,128)(2,1)} async-done(((bf16[512,512]{1,0:T(8,128)(2,1)}), bf16[2048,512]{1,0:T(8,128)(2,1)}) %all-gather.19.cloned.1.call-update) | async-done | bytes 2097168 | tf_op jit(solution)/shard_map/all_gather | solution.py:150
  47.6 32.9 %all-gather.21.cloned.1.call-done = bf16[2048,512]{1,0:T(8,128)(2,1)} async-done(((bf16[512,512]{1,0:T(8,128)(2,1)}), bf16[2048,512]{1,0:T(8,128)(2,1)}) %all-gather.21.cloned.1.call-update) | async-done | bytes 2097168 | tf_op jit(solution)/shard_map/all_gather | solution.py:151
  90.6 3.0 fusion.55
  93.6 3.0 convolution_select_fusion.2
  105.1 2.2 convolution_add_fusion.3
  107.3 4.0 convolution_select_fusion.1
  114.5 3.2 convolution_add_fusion.2
  122.0 4.2 fusion.46
  126.3 5.0 %multiply_add_fusion = f32[2,8,4,64,64]{4,3,2,1,0:T(8,128)S(1)} fusion(f32[2,8,4,32,64]{4,3,2,1,0:T(8,128)S(1)} %convolution_negate_fusion.1, f32[2,8,4,64]{3,2,1,0:T(4,128)S(1)} %copy-done.59, f32[64,64]{1,0:T(8,128)S(1)} %fusion.167, f32[2,8,4,32,64]{4,1,2,3,0:T(8,128)} %copy-done.15), kind=kOutput, calls=%fused_computation.8 | convolution fusion | flops 101187584 | bytes 2129920 | tf_op jit(solution)/shard_map/...sk,...sj->...kj/dot_general | solution.py:66
  133.3 4.0 convolution_add_fusion.1
  145.7 11.3 %pad.33 = f32[2,8,4,64,64]{4,3,2,1,0:T(8,128)} pad(f32[2,8,2,64,64]{4,3,2,1,0:T(8,128)S(1)} %copy-done.30, f32[]{:T(128)} %constant.27.clone.1), padding=0_0_0x0_0_0x1_0_1x0_0_0x0_0_0 | pad | bytes 1572868 | tf_op jit(solution)/shard_map/pad | solution.py:212
  157.1 11.2 %pad.32 = f32[2,8,4,64,64]{4,3,2,1,0:T(8,128)} pad(f32[2,8,2,64,64]{4,3,2,1,0:T(8,128)S(1)} %pad_maximum_fusion.1, f32[]{:T(128)} %constant.27.clone.1), padding=0_0_0x0_0_0x0_1_1x0_0_0x0_0_0 | pad | bytes 1572868 | tf_op jit(solution)/shard_map/pad | solution.py:212
  168.3 11.2 %pad.28 = f32[2,8,4,64,64]{4,3,2,1,0:T(8,128)} pad(f32[2,8,2,64,64]{4,3,2,1,0:T(8,128)S(1)} %pad_maximum_fusion, f32[]{:T(128)} %constant.27.clone.1), padding=0_0_0x0_0_0x0_1_1x0_0_0x0_0_0 | pad | bytes 1572868 | tf_op jit(solution)/shard_map/pad | solution.py:212
  179.6 16.7 %pad.29 = f32[2,8,4,64,64]{4,3,2,1,0:T(8,128)} pad(f32[2,8,2,64,64]{4,3,2,1,0:T(8,128)} %pad_add_fusion.1, f32[]{:T(128)} %constant.27.clone.1), padding=0_0_0x0_0_0x1_0_1x0_0_0x0_0_0 | pad | bytes 1572868 | tf_op jit(solution)/shard_map/pad | solution.py:212
  196.3 2.2 add_convert_fusion
  198.5 10.7 %all-gather.6 = bf16[4,8,1,64,64]{4,3,2,1,0:T(8,128)(2,1)S(1)} all-gather(bf16[1,8,1,64,64]{4,3,2,1,0:T(8,128)(2,1)S(1)} %get-tuple-element.24), channel_id=8, replica_groups=mesh['sp_0'=8,'sp_1'=4,'fs'=4,'tp'=2] {'sp_1'}, dimensions={0}, use_global_device_ids=true | all-gather | bytes 327680 | tf_op jit(solution)/shard_map/all_gather | solution.py:33
  211.1 11.9 %all-gather.4 = bf16[4,8,1,64,64]{4,3,2,1,0:T(8,128)(2,1)S(1)} all-gather(bf16[1,8,1,64,64]{4,3,2,1,0:T(8,128)(2,1)S(1)} %get-tuple-element.22), channel_id=6, replica_groups=mesh['sp_0'=8,'sp_1'=4,'fs'=4,'tp'=2] {'sp_1'}, dimensions={0}, use_global_device_ids=true | all-gather | bytes 327680 | tf_op jit(solution)/shard_map/all_gather | solution.py:33
  225.7 22.8 %all-gather.7 = bf16[64,64,64]{2,1,0:T(8,128)(2,1)S(1)} all-gather(bf16[8,64,64]{2,1,0:T(8,128)(2,1)S(1)} %get-tuple-element.46), channel_id=9, replica_groups=mesh['sp_0'=8,'sp_1'=4,'fs'=4,'tp'=2] {'sp_0'}, dimensions={0}, use_global_device_ids=true | all-gather | bytes 589824 | tf_op jit(solution)/shard_map/all_gather | solution.py:33
  249.3 22.2 %all-gather.5 = bf16[64,64,64]{2,1,0:T(8,128)(2,1)S(1)} all-gather(bf16[8,64,64]{2,1,0:T(8,128)(2,1)S(1)} %get-tuple-element.48), channel_id=7, replica_groups=mesh['sp_0'=8,'sp_1'=4,'fs'=4,'tp'=2] {'sp_0'}, dimensions={0}, use_global_device_ids=true | all-gather | bytes 589824 | tf_op jit(solution)/shard_map/all_gather | solution.py:33
  273.1 10.5 %all-gather.2 = bf16[4,8,1,64,64]{4,3,2,1,0:T(8,128)(2,1)S(1)} all-gather(bf16[1,8,1,64,64]{4,3,2,1,0:T(8,128)(2,1)S(1)} %get-tuple-element.23), channel_id=4, replica_groups=mesh['sp_0'=8,'sp_1'=4,'fs'=4,'tp'=2] {'sp_1'}, dimensions={0}, use_global_device_ids=true | all-gather | bytes 327680 | tf_op jit(solution)/shard_map/all_gather | solution.py:33
  283.6 10.3 %all-gather = bf16[4,8,1,64,64]{4,3,2,1,0:T(8,128)(2,1)S(1)} all-gather(bf16[1,8,1,64,64]{4,3,2,1,0:T(8,128)(2,1)S(1)} %get-tuple-element.21), channel_id=2, replica_groups=mesh['sp_0'=8,'sp_1'=4,'fs'=4,'tp'=2] {'sp_1'}, dimensions={0}, use_global_device_ids=true | all-gather | bytes 327680 | tf_op jit(solution)/shard_map/all_gather | solution.py:33
  295.9 20.4 %all-gather.3 = bf16[64,64,64]{2,1,0:T(8,128)(2,1)S(1)} all-gather(bf16[8,64,64]{2,1,0:T(8,128)(2,1)S(1)} %get-tuple-element.50), channel_id=5, replica_groups=mesh['sp_0'=8,'sp_1'=4,'fs'=4,'tp'=2] {'sp_0'}, dimensions={0}, use_global_device_ids=true | all-gather | bytes 589824 | tf_op jit(solution)/shard_map/all_gather | solution.py:33
  317.2 21.5 %all-gather.1 = bf16[64,64,64]{2,1,0:T(8,128)(2,1)S(1)} all-gather(bf16[8,64,64]{2,1,0:T(8,128)(2,1)S(1)} %get-tuple-element.52), channel_id=3, replica_groups=mesh['sp_0'=8,'sp_1'=4,'fs'=4,'tp'=2] {'sp_0'}, dimensions={0}, use_global_device_ids=true | all-gather | bytes 589824 | tf_op jit(solution)/shard_map/all_gather | solution.py:33
  345.2 3.0 fusion.30
  363.4 3.1 convolution_select_fusion.3
  367.7 3.1 convolution_select_fusion
  376.6 3.4 fusion.9
  386.4 5.5 %collective-permute-start = (bf16[8,512]{1,0:T(8,128)(2,1)S(1)}, bf16[8,512]{1,0:T(8,128)(2,1)S(1)}, u32[]{:S(2)}, u32[]{:S(2)}) collective-permute-start(bf16[8,512]{1,0:T(8,128)(2,1)S(1)} %get-tuple-element.34), channel_id=1, source_target_pairs={{0,8},{8,16},{16,24},{24,32},{32,40},{40,48},{48,56},{56,64},{64,7... | collective-permute-start | bytes 24584 | tf_op jit(solution)/shard_map/ppermute | solution.py:56
  391.9 35.5 %all_to_all.32 = bf16[2,64,512]{2,1,0:T(8,128)(2,1)S(1)} all-to-all(bf16[2,64,512]{2,1,0:T(8,128)(2,1)S(1)} %multiply_convert_fusion), channel_id=1, replica_groups=mesh['sp_0'=8,'sp_1'=4,'fs'=4,'tp'=2] {'tp'}, dimensions={0} | all-to-all | bytes 262144 | tf_op jit(solution)/shard_map/all_to_all | solution.py:278
  429.2 3.9 all_to_all.33
  433.1 3.6 fusion.222
  436.7 4.3 fusion.1
  (338 shorter events, 95.7 us)
Async XLA Ops:
  6.5 5.0 %copy-start = (bf16[2048,128]{1,0:T(8,128)(2,1)S(1)}, bf16[2048,128]{1,0:T(8,128)(2,1)}, u32[]{:S(2)}) copy-start(bf16[2048,128]{1,0:T(8,128)(2,1)} %param.24) | copy-start | bytes 1572868
  6.5 4.7 %copy-start.68 = (f32[2,512]{1,0:T(2,128)S(1)}, f32[2,512]{1,0:T(2,128)}, u32[]{:S(2)}) copy-start(f32[2,512]{1,0:T(2,128)} %param.26) | copy-start | bytes 12292
  6.5 4.7 %copy-start.67 = (bf16[2048]{0:T(1024)(128)(2,1)S(1)}, bf16[2048]{0:T(1024)(128)(2,1)}, u32[]{:S(2)}) copy-start(bf16[2048]{0:T(1024)(128)(2,1)} %param.19) | copy-start | bytes 12292
  6.5 4.7 %copy-start.5 = (bf16[1,128,2048]{2,1,0:T(8,128)(2,1)S(1)}, bf16[1,128,2048]{2,1,0:T(8,128)(2,1)}, u32[]{:S(2)}) copy-start(bf16[1,128,2048]{2,1,0:T(8,128)(2,1)} %param.18) | copy-start | bytes 1572868
  6.5 38.7 %all-gather.19.cloned.1.call-start = ((), (), s32[]{:S(2)}) async-start(), calls=%async_computation.3 | async-start | bytes 2621440 | tf_op jit(solution)/shard_map/all_gather | solution.py:150
  7.3 73.2 %all-gather.21.cloned.1.call-start = ((), (), s32[]{:S(2)}) async-start(), calls=%async_computation.4 | async-start | bytes 2621440 | tf_op jit(solution)/shard_map/all_gather | solution.py:151
  8.0 337.1 %all-gather.17.cloned.1.call-start = ((), (), s32[]{:S(2)}) async-start(), calls=%async_computation.2 | async-start | bytes 2621440 | tf_op jit(solution)/shard_map/all_gather | solution.py:149
  8.8 339.4 %all-gather.23.cloned.1.call-start = ((), (), s32[]{:S(2)}) async-start(), calls=%async_computation.5 | async-start | bytes 2621440 | tf_op jit(solution)/shard_map/all_gather | solution.py:153
  9.3 372.0 %all-gather.29.cloned.1.call-start = ((), (), s32[]{:S(2)}) async-start(), calls=%async_computation.8 | async-start | bytes 2621440 | tf_op jit(solution)/shard_map/all_gather | solution.py:154
  10.0 372.0 %all-gather.27.cloned.1.call-start = ((), (), s32[]{:S(2)}) async-start(), calls=%async_computation.7 | async-start | bytes 2621440 | tf_op jit(solution)/shard_map/all_gather | solution.py:152
  10.5 422.6 %all-gather.25.cloned.1.call-start = ((), (), s32[]{:S(2)}) async-start(), calls=%async_computation.6 | async-start | bytes 6291456 | tf_op jit(solution)/shard_map/all_gather | solution.py:282
  11.5 69.0 %copy-start.62 = (f32[128]{0:T(128)}, f32[128]{0:T(128)S(1)}, u32[]{:S(2)}) copy-start(f32[128]{0:T(128)S(1)} %add_rsqrt_fusion.2) | copy-start | bytes 1540
  93.6 13.7 %copy-start.7 = (f32[2,8,4,32,64]{4,1,2,3,0:T(8,128)}, f32[2,8,4,32,64]{4,1,2,3,0:T(8,128)S(1)}, u32[]{:S(2)}) copy-start(f32[2,8,4,32,64]{4,1,2,3,0:T(8,128)S(1)} %get-tuple-element.12) | copy-start | bytes 1572868
  93.6 28.4 %copy-start.15 = (f32[2,8,4,32,64]{4,1,2,3,0:T(8,128)}, f32[2,8,4,32,64]{4,1,2,3,0:T(8,128)S(1)}, u32[]{:S(2)}) copy-start(f32[2,8,4,32,64]{4,1,2,3,0:T(8,128)S(1)} %get-tuple-element.16) | copy-start | bytes 1572868
  114.5 17.9 %copy-start.22 = (f32[1,4,32,8,64]{4,2,1,3,0:T(8,128)}, f32[1,4,32,8,64]{4,2,1,3,0:T(8,128)S(1)}, u32[]{:S(2)}) copy-start(f32[1,4,32,8,64]{4,2,1,3,0:T(8,128)S(1)} %copy.129) | copy-start | bytes 786436
  119.6 6.7 %copy-start.11 = (f32[2,8,4,32,64]{4,3,2,1,0:T(8,128)}, f32[2,8,4,32,64]{4,3,2,1,0:T(8,128)S(1)}, u32[]{:S(2)}) copy-start(f32[2,8,4,32,64]{4,3,2,1,0:T(8,128)S(1)} %convolution_negate_fusion.1) | copy-start | bytes 1572868
  131.3 11.3 %copy-start.2 = (f32[2,8,4,64,64]{4,3,2,1,0:T(8,128)}, f32[2,8,4,64,64]{4,3,2,1,0:T(8,128)S(1)}, u32[]{:S(2)}) copy-start(f32[2,8,4,64,64]{4,3,2,1,0:T(8,128)S(1)} %multiply_add_fusion) | copy-start | bytes 3145732
  145.6 11.3 %slice-start.1 = ((f32[2,8,4,64,64]{4,3,2,1,0:T(8,128)}), f32[2,8,1,64,64]{4,3,2,1,0:T(8,128)S(1)}, s32[]{:S(2)}) async-start(f32[2,8,4,64,64]{4,3,2,1,0:T(8,128)} %copy-done.16), calls=%async_computation.11 | async-start | bytes 1048576 | tf_op jit(solution)/shard_map/slice | solution.py:212
  145.7 11.3 %copy-start.53 = (f32[2,8,1,64,64]{4,3,2,1,0:T(8,128)S(1)}, f32[2,8,1,64,64]{4,3,2,1,0:T(8,128)}, u32[]{:S(2)}) copy-start(f32[2,8,1,64,64]{4,3,2,1,0:T(8,128)} %fusion.13) | copy-start | bytes 786436
  157.0 11.2 %slice-start = ((f32[2,8,4,64,64]{4,3,2,1,0:T(8,128)}), f32[2,8,1,64,64]{4,3,2,1,0:T(8,128)S(1)}, s32[]{:S(2)}) async-start(f32[2,8,4,64,64]{4,3,2,1,0:T(8,128)} %copy-done.2), calls=%async_computation.10 | async-start | bytes 1048576 | tf_op jit(solution)/shard_map/slice | solution.py:212
  157.0 11.2 %copy-start.54 = (f32[2,8,1,64,64]{4,3,2,1,0:T(8,128)S(1)}, f32[2,8,1,64,64]{4,3,2,1,0:T(8,128)}, u32[]{:S(2)}) copy-start(f32[2,8,1,64,64]{4,3,2,1,0:T(8,128)} %convolution_bitcast_fusion.3) | copy-start | bytes 786436
  179.6 16.7 %copy-start.3 = (f32[2,8,4,64,64]{4,3,2,1,0:T(8,128)S(1)}, f32[2,8,4,64,64]{4,3,2,1,0:T(8,128)}, u32[]{:S(2)}) copy-start(f32[2,8,4,64,64]{4,3,2,1,0:T(8,128)} %pad.33) | copy-start | bytes 3145732
  196.3 12.9 %copy-start.18 = (f32[2,8,4,64,64]{4,3,2,1,0:T(8,128)S(1)}, f32[2,8,4,64,64]{4,3,2,1,0:T(8,128)}, u32[]{:S(2)}) copy-start(f32[2,8,4,64,64]{4,3,2,1,0:T(8,128)} %pad.28) | copy-start | bytes 3145732
  196.3 12.9 %copy-start.19 = (f32[2,8,4,64,64]{4,3,2,1,0:T(8,128)S(1)}, f32[2,8,4,64,64]{4,3,2,1,0:T(8,128)}, u32[]{:S(2)}) copy-start(f32[2,8,4,64,64]{4,3,2,1,0:T(8,128)} %pad.29) | copy-start | bytes 3145732
  224.5 24.6 %copy-start.33 = (f32[8,64,64]{2,1,0:T(8,128)}, f32[8,64,64]{2,1,0:T(8,128)S(1)}, u32[]{:S(2)}) copy-start(f32[8,64,64]{2,1,0:T(8,128)S(1)} %convolution_add_fusion.19) | copy-start | bytes 393220
  224.8 24.6 %copy-start.34 = (f32[8,64,64]{2,1,0:T(8,128)}, f32[8,64,64]{2,1,0:T(8,128)S(1)}, u32[]{:S(2)}) copy-start(f32[8,64,64]{2,1,0:T(8,128)S(1)} %convolution_add_fusion.18) | copy-start | bytes 393220
  294.4 22.3 %copy-start.45 = (f32[8,64,64]{2,1,0:T(8,128)}, f32[8,64,64]{2,1,0:T(8,128)S(1)}, u32[]{:S(2)}) copy-start(f32[8,64,64]{2,1,0:T(8,128)S(1)} %convolution_add_fusion.33) | copy-start | bytes 393220
  316.4 24.8 %copy-start.26 = (bf16[64,64,64]{2,1,0:T(8,128)(2,1)}, bf16[64,64,64]{2,1,0:T(8,128)(2,1)S(1)}, u32[]{:S(2)}) copy-start(bf16[64,64,64]{2,1,0:T(8,128)(2,1)S(1)} %all-gather.3) | copy-start | bytes 1572868
  348.2 88.5 %all-gather.31.cloned.1.call-start = ((), (), s32[]{:S(2)}) async-start(), calls=%async_computation.9 | async-start | bytes 6291456 | tf_op jit(solution)/shard_map/all_gather | solution.py:283
  381.8 10.1 %copy-start.64 = (f32[512]{0:T(512)S(1)}, f32[512]{0:T(512)}, u32[]{:S(2)}) copy-start(f32[512]{0:T(512)} %convert_element_type.431) | copy-start | bytes 6148
  384.5 43.0 %collective-permute-start.1 = (bf16[8,512]{1,0:T(8,128)(2,1)S(1)}, bf16[8,512]{1,0:T(8,128)(2,1)S(1)}, u32[]{:S(2)}, u32[]{:S(2)}) collective-permute-start(bf16[8,512]{1,0:T(8,128)(2,1)S(1)} %get-tuple-element.35), channel_id=1, source_target_pairs={{8,0},{16,8},{24,16},{32,24},{40,32},{48,40},{56,48},{64,56},{72,6... | collective-permute-start | bytes 24584 | tf_op jit(solution)/shard_map/ppermute | solution.py:58
  386.4 41.1 %collective-permute-start = (bf16[8,512]{1,0:T(8,128)(2,1)S(1)}, bf16[8,512]{1,0:T(8,128)(2,1)S(1)}, u32[]{:S(2)}, u32[]{:S(2)}) collective-permute-start(bf16[8,512]{1,0:T(8,128)(2,1)S(1)} %get-tuple-element.34), channel_id=1, source_target_pairs={{0,8},{8,16},{16,24},{24,32},{32,40},{40,48},{48,56},{56,64},{64,7... | collective-permute-start | bytes 24584 | tf_op jit(solution)/shard_map/ppermute | solution.py:56
  (56 other events, 120.3 us)
Sparse Core Ops, SparseCore 0:
  9.2 36.0 all-gather.18
  47.1 33.3 all-gather.20
  82.3 33.3 all-gather.16
  117.4 33.3 all-gather.22
  152.5 33.3 all-gather.28
  187.5 33.3 all-gather.26
  348.3 47.0 all-gather.24
  397.2 31.7 all-gather.30
where the time goes:
time: 454 us; the launch traced here: 448 us
  blocking collectives  170 us (37%)
  matrix products  97.3 us (21%)
  local copies, waits for them, and re-layouts  78.8 us (17%)
  waiting for transfers between devices  63.8 us (14%)
  between operations  15.5 us (3%)
  other arithmetic  15 us (3%)
  starting transfers between devices  8.1 us (2%)
    all_gather x8, blocking collectives, prefix_by_axis(): lax.all_gather(part.astype(kind), axis)  130 us
    dot_general x67, matrix products, contract(): return jnp.einsum(form, left, right, precision=highest)  77.8 us
    pad x4, local copies, waits for them, and re-layouts, shards(): lax.associative_scan(chain_combine, (transfer, carried), axis=2)  50.4 us
    all_to_all x1, blocking collectives, shards(): lax.all_to_all(attn_out, 'tp', split_axis=0, concat_axis=1, tiled=True)  35.5 us
    all_gather x1, waiting for transfers between devices, shards(): lax.all_gather(value_matrix, 'fs', axis=0, tiled=True)  32.9 us
    all_gather x1, waiting for transfers between devices, shards(): lax.all_gather(key_matrix, 'fs', axis=0, tiled=True)  27.2 us
    dot_general x6, matrix products, project(): jnp.dot(left, weight, preferred_element_type=jnp.float32)  10 us
    rev x12, local copies, waits for them, and re-layouts, both_ways(): stacked = jnp.stack([forward, jnp.flip(backward, axis=0)], axis=0)  9.63 us
  transfers between devices with their start and end apart: 10, of which 2 were waited for; matrix products, arithmetic and copies ran while one was open for 40% of the time, Pallas kernels for 0%

commit v1 on v0

--- a/solution.py
+++ b/solution.py
@@ -16,6 +16,13 @@
 unit_eps = 1e-06
 span_len = 32
 highest = lax.Precision.HIGHEST
+
+
+def all_by_exchange(x, axis, dim):
+    size = lax.axis_size(axis)
+    blocks = jnp.stack([x for _ in range(size)])
+    blocks = lax.all_to_all(blocks, axis, split_axis=0, concat_axis=0)
+    return jnp.concatenate(blocks, axis=dim)
 
 
 def filled_with(shard, identity):
@@ -148,7 +155,7 @@
     recept_full, key_full, value_full, pool_full, attn_full, pool_back = (
         lax.all_gather(receptance_matrix, "fs", axis=0, tiled=True),
         lax.all_gather(key_matrix, "fs", axis=0, tiled=True),
-        lax.all_gather(value_matrix, "fs", axis=0, tiled=True),
+        all_by_exchange(value_matrix, "fs", 0),
         lax.all_gather(pooling_input_weight, "fs", axis=0, tiled=True),
         lax.all_gather(attention_output_matrix, "fs", axis=0, tiled=True),
         lax.all_gather(pooling_output_matrix, "fs", axis=0, tiled=True),

time: 454 us -> 429 us (0.945)
  waiting for transfers between devices: 63.8 us -> 32.8 us
  matrix products: 97.3 us -> 90.9 us
  blocking collectives: 170 us -> 175 us
    all_gather x1 -> x0, waiting for transfers between devices: 32.9 us -> none  [shards(): lax.all_gather(value_matrix, 'fs', axis=0, tiled=True)]
    all_to_all x0 -> x1, waiting for transfers between devices: none -> 28.8 us  [all_by_exchange(): blocks = lax.all_to_all(blocks, axis, split_axis=0, concat_axis=0)]
    all_gather x1, waiting for transfers between devices: 27.2 us -> 0.71 us  [shards(): lax.all_gather(key_matrix, 'fs', axis=0, tiled=True)]
    dot_general x67, matrix products: 77.8 us -> 71.4 us  [contract(): return jnp.einsum(form, left, right, precision=highest)]
    all_to_all x0 -> x1, starting transfers between devices: none -> 4.59 us  [all_by_exchange(): blocks = lax.all_to_all(blocks, axis, split_axis=0, concat_axis=0)]
  transfers between devices with their start and end apart: 10 -> 10, of which waited for: 2 -> 2; matrix products, arithmetic and copies ran while one was open for 40% -> 42% of each run, Pallas kernels for 0% -> 0%
where the time goes in v1:
time: 429 us; the launch traced here: 423 us
  blocking collectives  175 us (41%)
  matrix products  90.9 us (21%)
  local copies, waits for them, and re-layouts  81.4 us (19%)
  waiting for transfers between devices  32.8 us (8%)
  between operations  15.6 us (4%)
  other arithmetic  15.1 us (4%)
  starting transfers between devices  12.6 us (3%)
    all_gather x8, blocking collectives, prefix_by_axis(): lax.all_gather(part.astype(kind), axis)  131 us
    dot_general x67, matrix products, contract(): return jnp.einsum(form, left, right, precision=highest)  71.4 us
    pad x4, local copies, waits for them, and re-layouts, shards(): lax.associative_scan(chain_combine, (transfer, carried), axis=2)  50.4 us
    all_to_all x1, blocking collectives, shards(): lax.all_to_all(attn_out, 'tp', split_axis=0, concat_axis=1, tiled=True)  39.9 us
    all_to_all x1, waiting for transfers between devices, all_by_exchange(): blocks = lax.all_to_all(blocks, axis, split_axis=0, concat_axis=0)  28.8 us
    rev x12, local copies, waits for them, and re-layouts, both_ways(): stacked = jnp.stack([forward, jnp.flip(backward, axis=0)], axis=0)  10.5 us
    dot_general x6, matrix products, project(): jnp.dot(left, weight, preferred_element_type=jnp.float32)  10 us
  transfers between devices with their start and end apart: 10, of which 2 were waited for; matrix products, arithmetic and copies ran while one was open for 42% of the time, Pallas kernels for 0%

profile of v1, /device:TPU:7, one launch (start us, length us, event | category | flops | bytes accessed | tf_op | source)
XLA Modules:
  0.0 423.5 jit_solution(6375265814943166524)
XLA Ops:
  10.9 4.6 %all-to-all-start = ((bf16[4,512,512]{2,1,0:T(8,128)(2,1)}), bf16[4,512,512]{2,1,0:T(8,128)(2,1)}, u32[]{:S(2)}, u32[]{:S(2)}) async-start(bf16[4,512,512]{2,1,0:T(8,128)(2,1)} %stack.93), calls=%async_computation | async-start | bytes 4194304 | tf_op jit(solution)/shard_map/all_to_all | solution.py:24
  24.8 28.8 %all-to-all-done = bf16[4,512,512]{2,1,0:T(8,128)(2,1)} async-done(((bf16[4,512,512]{2,1,0:T(8,128)(2,1)}), bf16[4,512,512]{2,1,0:T(8,128)(2,1)}, u32[]{:S(2)}, u32[]{:S(2)}) %all-to-all-start) | async-done | bytes 2097184 | tf_op jit(solution)/shard_map/all_to_all | solution.py:24
  53.6 2.1 fusion.30
  73.2 3.0 convolution_select_fusion.2
  84.9 3.0 convolution_select_fusion.1
  93.3 4.2 fusion.50
  97.5 3.7 multiply_add_fusion
  103.2 4.0 convolution_add_fusion.1
  115.6 11.3 %pad.33 = f32[2,8,4,64,64]{4,3,2,1,0:T(8,128)} pad(f32[2,8,2,64,64]{4,3,2,1,0:T(8,128)S(1)} %copy-done.29, f32[]{:T(128)} %constant.27.clone.1), padding=0_0_0x0_0_0x1_0_1x0_0_0x0_0_0 | pad | bytes 1572868 | tf_op jit(solution)/shard_map/pad | solution.py:219
  127.0 11.2 %pad.32 = f32[2,8,4,64,64]{4,3,2,1,0:T(8,128)} pad(f32[2,8,2,64,64]{4,3,2,1,0:T(8,128)S(1)} %pad_maximum_fusion.1, f32[]{:T(128)} %constant.27.clone.1), padding=0_0_0x0_0_0x0_1_1x0_0_0x0_0_0 | pad | bytes 1572868 | tf_op jit(solution)/shard_map/pad | solution.py:219
  138.3 11.2 %pad.28 = f32[2,8,4,64,64]{4,3,2,1,0:T(8,128)} pad(f32[2,8,2,64,64]{4,3,2,1,0:T(8,128)S(1)} %pad_maximum_fusion, f32[]{:T(128)} %constant.27.clone.1), padding=0_0_0x0_0_0x0_1_1x0_0_0x0_0_0 | pad | bytes 1572868 | tf_op jit(solution)/shard_map/pad | solution.py:219
  149.6 16.7 %pad.29 = f32[2,8,4,64,64]{4,3,2,1,0:T(8,128)} pad(f32[2,8,2,64,64]{4,3,2,1,0:T(8,128)} %pad_add_fusion.1, f32[]{:T(128)} %constant.27.clone.1), padding=0_0_0x0_0_0x1_0_1x0_0_0x0_0_0 | pad | bytes 1572868 | tf_op jit(solution)/shard_map/pad | solution.py:219
  166.3 2.2 add_convert_fusion
  168.5 9.9 %all-gather.6 = bf16[4,8,1,64,64]{4,3,2,1,0:T(8,128)(2,1)S(1)} all-gather(bf16[1,8,1,64,64]{4,3,2,1,0:T(8,128)(2,1)S(1)} %get-tuple-element.24), channel_id=8, replica_groups=mesh['sp_0'=8,'sp_1'=4,'fs'=4,'tp'=2] {'sp_1'}, dimensions={0}, use_global_device_ids=true | all-gather | bytes 327680 | tf_op jit(solution)/shard_map/all_gather | solution.py:40
  180.3 11.1 %all-gather.4 = bf16[4,8,1,64,64]{4,3,2,1,0:T(8,128)(2,1)S(1)} all-gather(bf16[1,8,1,64,64]{4,3,2,1,0:T(8,128)(2,1)S(1)} %get-tuple-element.22), channel_id=6, replica_groups=mesh['sp_0'=8,'sp_1'=4,'fs'=4,'tp'=2] {'sp_1'}, dimensions={0}, use_global_device_ids=true | all-gather | bytes 327680 | tf_op jit(solution)/shard_map/all_gather | solution.py:40
  194.2 26.6 %all-gather.7 = bf16[64,64,64]{2,1,0:T(8,128)(2,1)S(1)} all-gather(bf16[8,64,64]{2,1,0:T(8,128)(2,1)S(1)} %get-tuple-element.46), channel_id=9, replica_groups=mesh['sp_0'=8,'sp_1'=4,'fs'=4,'tp'=2] {'sp_0'}, dimensions={0}, use_global_device_ids=true | all-gather | bytes 589824 | tf_op jit(solution)/shard_map/all_gather | solution.py:40
  221.6 21.2 %all-gather.5 = bf16[64,64,64]{2,1,0:T(8,128)(2,1)S(1)} all-gather(bf16[8,64,64]{2,1,0:T(8,128)(2,1)S(1)} %get-tuple-element.48), channel_id=7, replica_groups=mesh['sp_0'=8,'sp_1'=4,'fs'=4,'tp'=2] {'sp_0'}, dimensions={0}, use_global_device_ids=true | all-gather | bytes 589824 | tf_op jit(solution)/shard_map/all_gather | solution.py:40
  244.4 10.5 %all-gather.2 = bf16[4,8,1,64,64]{4,3,2,1,0:T(8,128)(2,1)S(1)} all-gather(bf16[1,8,1,64,64]{4,3,2,1,0:T(8,128)(2,1)S(1)} %get-tuple-element.23), channel_id=4, replica_groups=mesh['sp_0'=8,'sp_1'=4,'fs'=4,'tp'=2] {'sp_1'}, dimensions={0}, use_global_device_ids=true | all-gather | bytes 327680 | tf_op jit(solution)/shard_map/all_gather | solution.py:40
  254.9 9.9 %all-gather = bf16[4,8,1,64,64]{4,3,2,1,0:T(8,128)(2,1)S(1)} all-gather(bf16[1,8,1,64,64]{4,3,2,1,0:T(8,128)(2,1)S(1)} %get-tuple-element.21), channel_id=2, replica_groups=mesh['sp_0'=8,'sp_1'=4,'fs'=4,'tp'=2] {'sp_1'}, dimensions={0}, use_global_device_ids=true | all-gather | bytes 327680 | tf_op jit(solution)/shard_map/all_gather | solution.py:40
  266.8 20.6 %all-gather.3 = bf16[64,64,64]{2,1,0:T(8,128)(2,1)S(1)} all-gather(bf16[8,64,64]{2,1,0:T(8,128)(2,1)S(1)} %get-tuple-element.50), channel_id=5, replica_groups=mesh['sp_0'=8,'sp_1'=4,'fs'=4,'tp'=2] {'sp_0'}, dimensions={0}, use_global_device_ids=true | all-gather | bytes 589824 | tf_op jit(solution)/shard_map/all_gather | solution.py:40
  288.3 21.5 %all-gather.1 = bf16[64,64,64]{2,1,0:T(8,128)(2,1)S(1)} all-gather(bf16[8,64,64]{2,1,0:T(8,128)(2,1)S(1)} %get-tuple-element.52), channel_id=3, replica_groups=mesh['sp_0'=8,'sp_1'=4,'fs'=4,'tp'=2] {'sp_0'}, dimensions={0}, use_global_device_ids=true | all-gather | bytes 589824 | tf_op jit(solution)/shard_map/all_gather | solution.py:40
  316.2 3.0 fusion.32
  319.6 2.1 fusion.16
  334.4 3.1 convolution_select_fusion.3
  338.7 3.1 convolution_select_fusion
  347.6 3.4 fusion.9
  353.4 2.1 fusion.221
  357.4 5.5 %collective-permute-start = (bf16[8,512]{1,0:T(8,128)(2,1)S(1)}, bf16[8,512]{1,0:T(8,128)(2,1)S(1)}, u32[]{:S(2)}, u32[]{:S(2)}) collective-permute-start(bf16[8,512]{1,0:T(8,128)(2,1)S(1)} %get-tuple-element.34), channel_id=1, source_target_pairs={{0,8},{8,16},{16,24},{24,32},{32,40},{40,48},{48,56},{56,64},{64,7... | collective-permute-start | bytes 24584 | tf_op jit(solution)/shard_map/ppermute | solution.py:63
  363.0 39.9 %all_to_all.37 = bf16[2,64,512]{2,1,0:T(8,128)(2,1)S(1)} all-to-all(bf16[2,64,512]{2,1,0:T(8,128)(2,1)S(1)} %multiply_convert_fusion), channel_id=1, replica_groups=mesh['sp_0'=8,'sp_1'=4,'fs'=4,'tp'=2] {'tp'}, dimensions={0} | all-to-all | bytes 262144 | tf_op jit(solution)/shard_map/all_to_all | solution.py:285
  404.6 3.9 all_to_all.38
  408.5 3.6 fusion.229
  412.1 4.3 %fusion.1 = bf16[1,64,2048]{2,1,0:T(8,128)(2,1)} fusion(f32[64,2048]{1,0:T(8,128)S(1)} %fusion.229, bf16[64,1024]{1,0:T(8,128)(2,1)S(1)} %bitcast.409, bf16[2048,1024]{1,0:T(8,128)(2,1)} %all-gather.28.cloned.1.call-done), kind=kOutput, calls=%fused_computation.2 | convolution fusion | flops 268697600 | bytes 5111808 | tf_op jit(solution)/shard_map/dot_general | solution.py:85
  (340 shorter events, 96.8 us)
Async XLA Ops:
  6.5 9.9 %copy-start = (bf16[2048,128]{1,0:T(8,128)(2,1)S(1)}, bf16[2048,128]{1,0:T(8,128)(2,1)}, u32[]{:S(2)}) copy-start(bf16[2048,128]{1,0:T(8,128)(2,1)} %param.24) | copy-start | bytes 1572868
  6.5 52.6 %all-gather.18.cloned.1.call-start = ((), (), s32[]{:S(2)}) async-start(), calls=%async_computation.4 | async-start | bytes 2621440 | tf_op jit(solution)/shard_map/all_gather | solution.py:157
  7.3 308.9 %all-gather.16.cloned.1.call-start = ((), (), s32[]{:S(2)}) async-start(), calls=%async_computation.3 | async-start | bytes 2621440 | tf_op jit(solution)/shard_map/all_gather | solution.py:156
  8.0 311.1 %all-gather.20.cloned.1.call-start = ((), (), s32[]{:S(2)}) async-start(), calls=%async_computation.5 | async-start | bytes 2621440 | tf_op jit(solution)/shard_map/all_gather | solution.py:160
  8.7 343.6 %all-gather.26.cloned.1.call-start = ((), (), s32[]{:S(2)}) async-start(), calls=%async_computation.8 | async-start | bytes 2621440 | tf_op jit(solution)/shard_map/all_gather | solution.py:161
  10.9 5.4 %copy-start.68 = (bf16[2048]{0:T(1024)(128)(2,1)S(1)}, bf16[2048]{0:T(1024)(128)(2,1)}, u32[]{:S(2)}) copy-start(bf16[2048]{0:T(1024)(128)(2,1)} %param.19) | copy-start | bytes 12292
  10.9 5.4 %copy-start.5 = (bf16[1,128,2048]{2,1,0:T(8,128)(2,1)S(1)}, bf16[1,128,2048]{2,1,0:T(8,128)(2,1)}, u32[]{:S(2)}) copy-start(bf16[1,128,2048]{2,1,0:T(8,128)(2,1)} %param.18) | copy-start | bytes 1572868
  10.9 42.7 %all-to-all-start = ((bf16[4,512,512]{2,1,0:T(8,128)(2,1)}), bf16[4,512,512]{2,1,0:T(8,128)(2,1)}, u32[]{:S(2)}, u32[]{:S(2)}) async-start(bf16[4,512,512]{2,1,0:T(8,128)(2,1)} %stack.93), calls=%async_computation | async-start | bytes 4194304 | tf_op jit(solution)/shard_map/all_to_all | solution.py:24
  15.5 337.5 %all-gather.24.cloned.1.call-start = ((), (), s32[]{:S(2)}) async-start(), calls=%async_computation.7 | async-start | bytes 2621440 | tf_op jit(solution)/shard_map/all_gather | solution.py:159
  16.1 392.3 %all-gather.22.cloned.1.call-start = ((), (), s32[]{:S(2)}) async-start(), calls=%async_computation.6 | async-start | bytes 6291456 | tf_op jit(solution)/shard_map/all_gather | solution.py:289
  16.5 42.7 %copy-start.63 = (f32[128]{0:T(128)}, f32[128]{0:T(128)S(1)}, u32[]{:S(2)}) copy-start(f32[128]{0:T(128)S(1)} %add_rsqrt_fusion.2) | copy-start | bytes 1540
  21.9 33.8 %copy-start.25 = (f32[1,4,32,8,64]{4,3,1,2,0:T(8,128)}, f32[1,4,32,8,64]{4,3,1,2,0:T(8,128)S(1)}, u32[]{:S(2)}) copy-start(f32[1,4,32,8,64]{4,3,1,2,0:T(8,128)S(1)} %fusion.77) | copy-start | bytes 786436
  57.1 33.8 %copy-start.19 = (f32[128,8,64]{2,0,1:T(8,128)}, f32[128,8,64]{2,0,1:T(8,128)S(1)}, u32[]{:S(2)}) copy-start(f32[128,8,64]{2,0,1:T(8,128)S(1)} %copy.128) | copy-start | bytes 786436
  58.5 32.4 %copy-start.22 = (f32[1,4,32,8,64]{4,2,1,3,0:T(8,128)}, f32[1,4,32,8,64]{4,2,1,3,0:T(8,128)S(1)}, u32[]{:S(2)}) copy-start(f32[1,4,32,8,64]{4,2,1,3,0:T(8,128)S(1)} %copy.129) | copy-start | bytes 786436
  73.2 11.7 %copy-start.7 = (f32[2,8,4,32,64]{4,1,2,3,0:T(8,128)}, f32[2,8,4,32,64]{4,1,2,3,0:T(8,128)S(1)}, u32[]{:S(2)}) copy-start(f32[2,8,4,32,64]{4,1,2,3,0:T(8,128)S(1)} %get-tuple-element.12) | copy-start | bytes 1572868
  90.9 6.6 %copy-start.11 = (f32[2,8,4,32,64]{4,3,2,1,0:T(8,128)}, f32[2,8,4,32,64]{4,3,2,1,0:T(8,128)S(1)}, u32[]{:S(2)}) copy-start(f32[2,8,4,32,64]{4,3,2,1,0:T(8,128)S(1)} %convolution_negate_fusion.1) | copy-start | bytes 1572868
  101.3 11.3 %copy-start.2 = (f32[2,8,4,64,64]{4,3,2,1,0:T(8,128)}, f32[2,8,4,64,64]{4,3,2,1,0:T(8,128)S(1)}, u32[]{:S(2)}) copy-start(f32[2,8,4,64,64]{4,3,2,1,0:T(8,128)S(1)} %multiply_add_fusion) | copy-start | bytes 3145732
  115.6 11.3 %slice-start.1 = ((f32[2,8,4,64,64]{4,3,2,1,0:T(8,128)}), f32[2,8,1,64,64]{4,3,2,1,0:T(8,128)S(1)}, s32[]{:S(2)}) async-start(f32[2,8,4,64,64]{4,3,2,1,0:T(8,128)} %copy-done.15), calls=%async_computation.11 | async-start | bytes 1048576 | tf_op jit(solution)/shard_map/slice | solution.py:219
  115.6 11.3 %copy-start.53 = (f32[2,8,1,64,64]{4,3,2,1,0:T(8,128)S(1)}, f32[2,8,1,64,64]{4,3,2,1,0:T(8,128)}, u32[]{:S(2)}) copy-start(f32[2,8,1,64,64]{4,3,2,1,0:T(8,128)} %fusion.15) | copy-start | bytes 786436
  127.0 11.2 %slice-start = ((f32[2,8,4,64,64]{4,3,2,1,0:T(8,128)}), f32[2,8,1,64,64]{4,3,2,1,0:T(8,128)S(1)}, s32[]{:S(2)}) async-start(f32[2,8,4,64,64]{4,3,2,1,0:T(8,128)} %copy-done.2), calls=%async_computation.10 | async-start | bytes 1048576 | tf_op jit(solution)/shard_map/slice | solution.py:219
  127.0 11.2 %copy-start.54 = (f32[2,8,1,64,64]{4,3,2,1,0:T(8,128)S(1)}, f32[2,8,1,64,64]{4,3,2,1,0:T(8,128)}, u32[]{:S(2)}) copy-start(f32[2,8,1,64,64]{4,3,2,1,0:T(8,128)} %convolution_bitcast_fusion.3) | copy-start | bytes 786436
  149.6 16.7 %copy-start.3 = (f32[2,8,4,64,64]{4,3,2,1,0:T(8,128)S(1)}, f32[2,8,4,64,64]{4,3,2,1,0:T(8,128)}, u32[]{:S(2)}) copy-start(f32[2,8,4,64,64]{4,3,2,1,0:T(8,128)} %pad.33) | copy-start | bytes 3145732
  166.3 12.1 %copy-start.17 = (f32[2,8,4,64,64]{4,3,2,1,0:T(8,128)S(1)}, f32[2,8,4,64,64]{4,3,2,1,0:T(8,128)}, u32[]{:S(2)}) copy-start(f32[2,8,4,64,64]{4,3,2,1,0:T(8,128)} %pad.28) | copy-start | bytes 3145732
  166.3 12.1 %copy-start.18 = (f32[2,8,4,64,64]{4,3,2,1,0:T(8,128)S(1)}, f32[2,8,4,64,64]{4,3,2,1,0:T(8,128)}, u32[]{:S(2)}) copy-start(f32[2,8,4,64,64]{4,3,2,1,0:T(8,128)} %pad.29) | copy-start | bytes 3145732
  192.9 28.4 %copy-start.32 = (f32[8,64,64]{2,1,0:T(8,128)}, f32[8,64,64]{2,1,0:T(8,128)S(1)}, u32[]{:S(2)}) copy-start(f32[8,64,64]{2,1,0:T(8,128)S(1)} %convolution_add_fusion.19) | copy-start | bytes 393220
  193.2 28.4 %copy-start.33 = (f32[8,64,64]{2,1,0:T(8,128)}, f32[8,64,64]{2,1,0:T(8,128)S(1)}, u32[]{:S(2)}) copy-start(f32[8,64,64]{2,1,0:T(8,128)S(1)} %convolution_add_fusion.18) | copy-start | bytes 393220
  265.3 22.4 %copy-start.44 = (f32[8,64,64]{2,1,0:T(8,128)}, f32[8,64,64]{2,1,0:T(8,128)S(1)}, u32[]{:S(2)}) copy-start(f32[8,64,64]{2,1,0:T(8,128)S(1)} %convolution_add_fusion.33) | copy-start | bytes 393220
  287.5 24.8 %copy-start.27 = (bf16[64,64,64]{2,1,0:T(8,128)(2,1)}, bf16[64,64,64]{2,1,0:T(8,128)(2,1)S(1)}, u32[]{:S(2)}) copy-start(bf16[64,64,64]{2,1,0:T(8,128)(2,1)S(1)} %all-gather.3) | copy-start | bytes 1572868
  319.2 92.9 %all-gather.28.cloned.1.call-start = ((), (), s32[]{:S(2)}) async-start(), calls=%async_computation.9 | async-start | bytes 6291456 | tf_op jit(solution)/shard_map/all_gather | solution.py:290
  352.8 10.1 %copy-start.65 = (f32[512]{0:T(512)S(1)}, f32[512]{0:T(512)}, u32[]{:S(2)}) copy-start(f32[512]{0:T(512)} %convert_element_type.442) | copy-start | bytes 6148
  355.5 47.3 %collective-permute-start.1 = (bf16[8,512]{1,0:T(8,128)(2,1)S(1)}, bf16[8,512]{1,0:T(8,128)(2,1)S(1)}, u32[]{:S(2)}, u32[]{:S(2)}) collective-permute-start(bf16[8,512]{1,0:T(8,128)(2,1)S(1)} %get-tuple-element.35), channel_id=1, source_target_pairs={{8,0},{16,8},{24,16},{32,24},{40,32},{48,40},{56,48},{64,56},{72,6... | collective-permute-start | bytes 24584 | tf_op jit(solution)/shard_map/ppermute | solution.py:65
  357.4 45.4 %collective-permute-start = (bf16[8,512]{1,0:T(8,128)(2,1)S(1)}, bf16[8,512]{1,0:T(8,128)(2,1)S(1)}, u32[]{:S(2)}, u32[]{:S(2)}) collective-permute-start(bf16[8,512]{1,0:T(8,128)(2,1)S(1)} %get-tuple-element.34), channel_id=1, source_target_pairs={{0,8},{8,16},{16,24},{24,32},{32,40},{40,48},{48,56},{56,64},{64,7... | collective-permute-start | bytes 24584 | tf_op jit(solution)/shard_map/ppermute | solution.py:63
  (57 other events, 127.6 us)
Sparse Core Ops, SparseCore 0:
  9.1 49.9 all-gather.17
  61.0 34.2 all-gather.15
  97.1 33.3 all-gather.19
  132.1 33.3 all-gather.25
  167.2 33.3 all-gather.23
  319.3 51.1 all-gather.21
  372.3 31.7 all-gather.27
